TPU v7x, 32 devices: a whole 2x2x4 slice. The times are simulated.
32 devices in a mesh: sp: 8 (over z, x), tp: 4 (over y, core).
Axes of the slice: x: 2, y: 2, z: 4, core: 2. Of those that a mesh axis runs over, the one named last changes fastest.
Arguments:
- queries: bfloat16 [2048, 1024], P('sp', 'tp'), may hold values from -6 to 6
- keys: bfloat16 [2048, 1024], P('sp', 'tp'), may hold values from -6 to 6
- values: bfloat16 [2048, 2048], P('sp', 'tp'), may hold values from -6 to 6
- gate_code: bfloat16 [2048, 32], P('sp'), may hold values from -5.5 to 5.5
- gate_up: bfloat16 [32, 1024], P(None, 'tp'), may hold values from -1 to 1
- gate_bias: float32 [1024], P('tp'), as said below
- gla_gain: float32 [256], replicated, may hold values from 0.1 to 1.9
- conv_input: bfloat16 [2048, 2048], P('sp', 'tp'), may hold values from -6 to 6
- conv_gate: bfloat16 [2048, 2048], P('sp', 'tp'), may hold values from -6 to 6
- conv_taps: float32 [3, 2048], P(None, 'tp'), may hold values from -3.5 to 3.5
- out_gla: bfloat16 [2048, 2048], P('tp', 'sp'), may hold values from -0.09375 to 0.09375
- out_conv: bfloat16 [2048, 2048], P('tp', 'sp'), may hold values from -0.09375 to 0.09375
Outputs:
- mixed: bfloat16 [2048, 2048], P(('sp', 'tp'))
Inputs may be any that keep to these rules, and one draw needn't show every extreme that they name: `gate_bias`: every bias is at least 1.5, so every decay per step lies strictly between 0 and 1.
All inputs are finite; a program needn't handle non-finite values.
Results may differ from a plain program's by a relative error of at most 0.028.
Values may be sent and summed in bfloat16 or wider, within the bound.
A program may use at most 64 MiB of HBM per device.

v0:
```python
import jax
import jax.numpy as jnp
from jax import lax
from jax.sharding import PartitionSpec as P

KEY_WIDTH = 128
HEAD_V = 256
SEGMENT_LENGTH = 64


softness_divisor = 16.0
epsilon = 1.0


def for_sending(x):
    return jax.tree.map(lambda a: a.astype(jnp.bfloat16) if a.dtype == jnp.float32 else a, x)


def from_behind(x, axis, by):
    count = lax.axis_size(axis)
    pairs = [(i, i + by) for i in range(count) if 0 <= i + by < count]
    return lax.ppermute(x, axis, pairs)


def chain(earlier, latter):
    return (earlier[0] * latter[0], latter[0][..., None] * earlier[1] + latter[1])


def per_device(
    queries,
    keys,
    values,
    gate_code,
    gate_up,
    gate_bias,
    gla_gain,
    conv_input,
    conv_gate,
    conv_taps,
    out_gla,
    out_conv,
):
    row_count = queries.shape[0]
    segment_count = row_count // SEGMENT_LENGTH
    head_count = queries.shape[1] // KEY_WIDTH
    gate_score = jnp.dot(gate_code, gate_up, preferred_element_type=jnp.float32) + gate_bias
    decay_logarithm = (jax.nn.log_sigmoid(gate_score) / softness_divisor).reshape(
        segment_count, SEGMENT_LENGTH, head_count, KEY_WIDTH
    )
    inside = jnp.cumsum(decay_logarithm, axis=1)
    seg_total = inside[:, -1]
    key_blocks = keys.reshape(segment_count, SEGMENT_LENGTH, head_count, KEY_WIDTH)
    scaled_keys = (key_blocks * jnp.exp(seg_total[:, None] - inside)).astype(jnp.bfloat16)
    value_blocks = values.reshape(segment_count, SEGMENT_LENGTH, head_count, HEAD_V)
    update = jnp.einsum(
        "nshk,nshv->nhkv", scaled_keys, value_blocks, preferred_element_type=jnp.float32
    )
    through, local_state = lax.associative_scan(chain, (jnp.exp(seg_total), update), axis=0)
    device_decay = through[-1]
    device_state = local_state[-1]
    columns = lax.all_to_all(
        device_state[None].astype(jnp.bfloat16), "sp", split_axis=3, concat_axis=0, tiled=True
    ).astype(jnp.float32)
    decays = lax.all_gather(device_decay[None], "sp", axis=0, tiled=True)
    running = lax.associative_scan(chain, (decays, columns), axis=0)[1]
    before = jnp.concatenate([jnp.zeros_like(running[:1]), running[:-1]], axis=0)
    incoming = lax.all_to_all(
        for_sending(before), "sp", split_axis=0, concat_axis=3, tiled=True
    ).astype(before.dtype)[0]
    states = local_state + through[..., None] * incoming[None]
    query_blocks = queries.reshape(segment_count, SEGMENT_LENGTH, head_count, KEY_WIDTH)
    readout = jnp.einsum(
        "nshk,nhkv->nshv",
        query_blocks,
        states.astype(jnp.bfloat16),
        preferred_element_type=jnp.float32,
    )
    norm_scale = lax.rsqrt(jnp.mean(readout * readout, axis=-1, keepdims=True) + epsilon)
    gla_mix = (
        (readout * norm_scale * gla_gain)
        .astype(jnp.bfloat16)
        .reshape(row_count, head_count * HEAD_V)
    )
    reach_rows = conv_taps.shape[0] - 1
    earlier_rows = from_behind(conv_input[row_count - reach_rows :], "sp", 1)
    extended = jnp.concatenate([earlier_rows, conv_input], axis=0)
    convolved = jnp.zeros(conv_input.shape, jnp.float32)
    for offset in range(reach_rows + 1):
        convolved = convolved + conv_taps[offset] * extended[offset : offset + row_count]
    conv_mix = (conv_gate * convolved).astype(jnp.bfloat16)
    wide_gla, wide_conv = (
        lax.all_gather(out_gla, "sp", axis=1, tiled=True),
        lax.all_gather(out_conv, "sp", axis=1, tiled=True),
    )
    summed = jnp.dot(gla_mix, wide_gla, preferred_element_type=jnp.float32)
    return lax.psum_scatter(
        (summed + jnp.dot(conv_mix, wide_conv, preferred_element_type=jnp.float32)).astype(
            jnp.bfloat16
        ),
        "tp",
        scatter_dimension=0,
        tiled=True,
    )


def solution(mesh):
    in_specs = (
        P("sp", "tp"),
        P("sp", "tp"),
        P("sp", "tp"),
        P("sp", None),
        P(None, "tp"),
        P("tp"),
        P(),
        P("sp", "tp"),
        P("sp", "tp"),
        P(None, "tp"),
        P("tp", "sp"),
        P("tp", "sp"),
    )
    out_specs = P(("sp", "tp"), None)
    return jax.shard_map(
        per_device, mesh=mesh, in_specs=in_specs, out_specs=out_specs, check_vma=False
    )
```

profile of v0, /device:TPU:0, one launch (start us, length us, event | category | flops | bytes accessed | tf_op | source)
XLA Modules:
  0.0 149.3 jit_solution(18421803840476476254)
XLA Ops:
  6.5 0.0 copy-start
  6.5 0.0 copy-start.3
  6.5 0.0 all-gather.3.cloned.1.call-start
  6.5 0.7 all-gather.3.cloned.1.call-update
  7.3 0.0 copy-done
  7.3 1.1 fusion.9
  8.3 0.1 reshape.57
  8.5 1.0 reshape.61
  9.5 0.0 copy-done.3
  9.5 0.1 reshape.58
  9.6 0.1 fusion.33
  9.8 0.2 multiply_convert_fusion.3
  10.0 0.3 fusion.11
  10.3 0.1 slice_add_fusion
  10.5 0.1 fusion.28
  10.6 0.1 fusion.27
  10.7 0.1 pad.49
  10.9 0.1 pad.50
  11.1 0.8 copy.32
  11.9 7.3 %all-to-all-start = ((bf16[1,2,128,256]{2,1,0,3:T(2,128)(2,1)}), bf16[1,2,128,256]{2,1,0,3:T(2,128)(2,1)S(1)}, u32[]{:S(2)}, u32[]{:S(2)}) async-start(bf16[1,2,128,256]{2,1,0,3:T(2,128)(2,1)} %copy.32), calls=%async_computation | async-start | bytes 262144 | tf_op jit(solution)/shard_map/all_to_all | solution.py:61
  19.1 0.0 all-gather.5.cloned.1.call-start
  19.2 0.7 all-gather.5.cloned.1.call-update
  19.9 0.0 copy-start.5
  20.0 0.0 copy-start.7
  20.0 21.3 %all_gather.9 = f32[8,2,128]{2,1,0:T(2,128)S(1)} all-gather(f32[1,2,128]{2,1,0:T(2,128)S(1)} %slice_add_fusion.5), channel_id=1, replica_groups=mesh['sp'=8,'tp'=4] {'sp'}, dimensions={0}, use_global_device_ids=true | all-gather | bytes 9216 | tf_op jit(solution)/shard_map/all_gather | solution.py:64
  41.4 0.6 copy.35
  42.0 0.0 all-to-all-done
  42.0 0.0 copy-done.5
  42.0 0.0 copy-done.7
  42.1 0.0 copy-start.1
  42.3 0.1 pad.138
  42.4 0.0 copy-start.4
  42.5 0.0 copy-start.6
  42.5 0.0 copy-start.8
  42.5 0.0 copy-start.9
  42.5 0.7 fusion.18
  43.2 0.1 pad.74
  43.4 0.7 concatenate.22.clone
  44.1 3.4 %all-to-all-start.1 = ((bf16[8,2,128,32]{2,3,1,0:T(8,128)(2,1)}), bf16[8,2,128,32]{2,3,1,0:T(8,128)(2,1)S(1)}, u32[]{:S(2)}, u32[]{:S(2)}) async-start(bf16[8,2,128,32]{2,3,1,0:T(8,128)(2,1)} %concatenate.22.clone), calls=%async_computation.1 | async-start | bytes 262144 | tf_op jit(solution)/shard_map/all_to_all | solution.py:67
  47.5 0.0 reduce-scatter.2.cloned.1.call-start
  47.5 0.0 copy-done.1
  47.5 3.8 %collective-permute-start = (bf16[2,512]{1,0:T(2,128)(2,1)S(1)}, bf16[2,512]{1,0:T(2,128)(2,1)S(1)}, u32[]{:S(2)}, u32[]{:S(2)}) collective-permute-start(bf16[2,512]{1,0:T(2,128)(2,1)S(1)} %slice.187), channel_id=1, source_target_pairs={{0,4},{4,8},{8,12},{12,16},{16,20},{20,24},{24,28},{1,5},{5,9},{9,... | collective-permute-start | bytes 6152 | tf_op jit(solution)/shard_map/ppermute | solution.py:22
  51.3 0.0 copy-done.6
  51.3 0.0 copy-done.8
  51.3 0.0 copy-done.4
  51.4 0.0 copy-start.10
  51.4 0.0 copy-done.9
  51.4 5.2 %all-to-all-done.1 = bf16[8,2,128,32]{2,3,1,0:T(8,128)(2,1)S(1)} async-done(((bf16[8,2,128,32]{2,3,1,0:T(8,128)(2,1)}), bf16[8,2,128,32]{2,3,1,0:T(8,128)(2,1)S(1)}, u32[]{:S(2)}, u32[]{:S(2)}) %all-to-all-start.1) | async-done | bytes 131104 | tf_op jit(solution)/shard_map/all_to_all | solution.py:67
  56.7 0.1 copy.40
  56.8 0.5 multiply_reduce_fusion
  57.3 0.0 copy-done.10
  57.3 0.1 multiply_convert_fusion.1
  57.4 0.3 copy.42
  57.7 8.6 %all-gather.3.cloned.1.call-done = bf16[512,2048]{1,0:T(8,128)(2,1)} async-done(((bf16[512,256]{1,0:T(8,128)(2,1)}), bf16[512,2048]{1,0:T(8,128)(2,1)}) %all-gather.3.cloned.1.call-update) | async-done | bytes 2097168 | tf_op jit(solution)/shard_map/all_gather | solution.py:92
  66.3 0.0 copy-start.2
  66.3 2.3 %fusion.34 = f32[256,2048]{1,0:T(8,128)S(1)} fusion(bf16[256,512]{1,0:T(8,128)(2,1)S(1)} %bitcast.43, bf16[512,2048]{1,0:T(8,128)(2,1)} %all-gather.3.cloned.1.call-done), kind=kOutput, calls=%fused_computation.81 | convolution fusion | flops 536870912 | bytes 4456448 | tf_op jit(solution)/shard_map/dot_general | solution.py:95
  68.7 0.0 collective-permute-done
  68.7 47.5 %all-gather.5.cloned.1.call-done = bf16[512,2048]{1,0:T(8,128)(2,1)} async-done(((bf16[512,256]{1,0:T(8,128)(2,1)}), bf16[512,2048]{1,0:T(8,128)(2,1)}) %all-gather.5.cloned.1.call-update) | async-done | bytes 2097168 | tf_op jit(solution)/shard_map/all_gather | solution.py:93
  116.2 0.0 copy-done.2
  116.2 3.4 %fusion = bf16[256,2048]{1,0:T(8,128)(2,1)} fusion(f32[256,2048]{1,0:T(8,128)S(1)} %fusion.34, bf16[512,2048]{1,0:T(8,128)(2,1)} %all-gather.5.cloned.1.call-done, bf16[256,512]{1,0:T(8,128)(2,1)S(1)} %copy-done.1, bf16[256,512]{1,0:T(8,128)(2,1)S(1)} %copy-done.2, bf16[2,512]{1,0:T(2,128)(2,1)S(1)} %collective-permute-done, f32[512]{0:T(512)S(1)} %bitcast.48, ...), kind=kOutput, calls=%fused_computation.1 | convolution fusion | flops 540147712 | bytes 5775360 | tf_op jit(solution)/shard_map/dot_general | solution.py:97
  119.6 0.0 reduce-scatter.2.cloned.1.call-update
  119.6 23.1 %reduce-scatter.2.cloned.1.call-done = bf16[64,2048]{1,0:T(8,128)(2,1)} async-done(((bf16[256,2048]{1,0:T(8,128)(2,1)}), bf16[64,2048]{1,0:T(8,128)(2,1)}) %reduce-scatter.2.cloned.1.call-update) | async-done | bytes 262160 | tf_op jit(solution)/shard_map/reduce_scatter | solution.py:96
  (42 shorter events, 0.7 us)
Async XLA Ops:
  6.5 0.7 copy-start
  6.5 3.0 %copy-start.3 = (bf16[256,512]{1,0:T(8,128)(2,1)S(1)}, bf16[256,512]{1,0:T(8,128)(2,1)}, u32[]{:S(2)}) copy-start(bf16[256,512]{1,0:T(8,128)(2,1)} %param.14) | copy-start | bytes 786436
  6.5 59.8 %all-gather.3.cloned.1.call-start = ((), (), s32[]{:S(2)}) async-start(), calls=%async_computation.3 | async-start | bytes 2359296 | tf_op jit(solution)/shard_map/all_gather | solution.py:92
  11.9 30.1 %all-to-all-start = ((bf16[1,2,128,256]{2,1,0,3:T(2,128)(2,1)}), bf16[1,2,128,256]{2,1,0,3:T(2,128)(2,1)S(1)}, u32[]{:S(2)}, u32[]{:S(2)}) async-start(bf16[1,2,128,256]{2,1,0,3:T(2,128)(2,1)} %copy.32), calls=%async_computation | async-start | bytes 262144 | tf_op jit(solution)/shard_map/all_to_all | solution.py:61
  19.1 97.1 %all-gather.5.cloned.1.call-start = ((), (), s32[]{:S(2)}) async-start(), calls=%async_computation.4 | async-start | bytes 2359296 | tf_op jit(solution)/shard_map/all_gather | solution.py:93
  19.9 22.1 %copy-start.5 = (f32[4,2,128]{2,1,0:T(2,128)}, f32[4,2,128]{2,1,0:T(2,128)S(1)}, u32[]{:S(2)}) copy-start(f32[4,2,128]{2,1,0:T(2,128)S(1)} %pad.53) | copy-start | bytes 12292
  20.0 22.0 %copy-start.7 = (f32[4,2,128]{2,1,0:T(2,128)}, f32[4,2,128]{2,1,0:T(2,128)S(1)}, u32[]{:S(2)}) copy-start(f32[4,2,128]{2,1,0:T(2,128)S(1)} %pad.54) | copy-start | bytes 12292
  42.1 5.4 %copy-start.1 = (bf16[256,512]{1,0:T(8,128)(2,1)S(1)}, bf16[256,512]{1,0:T(8,128)(2,1)}, u32[]{:S(2)}) copy-start(bf16[256,512]{1,0:T(8,128)(2,1)} %param.19) | copy-start | bytes 786436
  42.4 8.9 %copy-start.4 = (bf16[256,256]{1,0:T(8,128)(2,1)S(1)}, bf16[256,256]{1,0:T(8,128)(2,1)}, u32[]{:S(2)}) copy-start(bf16[256,256]{1,0:T(8,128)(2,1)} %param.12) | copy-start | bytes 393220
  42.5 8.9 %copy-start.6 = (f32[4,2,128]{2,1,0:T(2,128)S(1)}, f32[4,2,128]{2,1,0:T(2,128)}, u32[]{:S(2)}) copy-start(f32[4,2,128]{2,1,0:T(2,128)} %copy-done.5) | copy-start | bytes 12292
  42.5 8.9 %copy-start.8 = (f32[4,2,128]{2,1,0:T(2,128)S(1)}, f32[4,2,128]{2,1,0:T(2,128)}, u32[]{:S(2)}) copy-start(f32[4,2,128]{2,1,0:T(2,128)} %copy-done.7) | copy-start | bytes 12292
  42.5 8.9 %copy-start.9 = (f32[3,512]{1,0:T(4,128)S(1)}, f32[3,512]{1,0:T(4,128)}, u32[]{:S(2)}) copy-start(f32[3,512]{1,0:T(4,128)} %param.21) | copy-start | bytes 18436
  44.1 12.6 %all-to-all-start.1 = ((bf16[8,2,128,32]{2,3,1,0:T(8,128)(2,1)}), bf16[8,2,128,32]{2,3,1,0:T(8,128)(2,1)S(1)}, u32[]{:S(2)}, u32[]{:S(2)}) async-start(bf16[8,2,128,32]{2,3,1,0:T(8,128)(2,1)} %concatenate.22.clone), calls=%async_computation.1 | async-start | bytes 262144 | tf_op jit(solution)/shard_map/all_to_all | solution.py:67
  47.5 95.3 %reduce-scatter.2.cloned.1.call-start = ((), (), s32[]{:S(2)}) async-start(), calls=%async_computation.5 | async-start | bytes 1310720 | tf_op jit(solution)/shard_map/reduce_scatter | solution.py:96
  47.5 21.1 %collective-permute-start = (bf16[2,512]{1,0:T(2,128)(2,1)S(1)}, bf16[2,512]{1,0:T(2,128)(2,1)S(1)}, u32[]{:S(2)}, u32[]{:S(2)}) collective-permute-start(bf16[2,512]{1,0:T(2,128)(2,1)S(1)} %slice.187), channel_id=1, source_target_pairs={{0,4},{4,8},{8,12},{12,16},{16,20},{20,24},{24,28},{1,5},{5,9},{9,... | collective-permute-start | bytes 6152 | tf_op jit(solution)/shard_map/ppermute | solution.py:22
  51.4 5.9 %copy-start.10 = (f32[256]{0:T(256)S(1)}, f32[256]{0:T(256)}, u32[]{:S(2)}) copy-start(f32[256]{0:T(256)} %param.18) | copy-start | bytes 3076
  66.3 49.9 %copy-start.2 = (bf16[256,512]{1,0:T(8,128)(2,1)S(1)}, bf16[256,512]{1,0:T(8,128)(2,1)}, u32[]{:S(2)}) copy-start(bf16[256,512]{1,0:T(8,128)(2,1)} %param.20) | copy-start | bytes 786436
Sparse Core Ops, SparseCore 0:
  9.4 56.8 all-gather.2
  68.4 47.8 all-gather.4
  119.7 22.9 reduce-scatter.1
where the time goes:
time: 150 us; the launch traced here: 149 us
  waiting for transfers between devices  85.9 us (57%)
  blocking collectives  21.3 us (14%)
  starting transfers between devices  14.5 us (10%)
  between operations  13.7 us (9%)
  matrix products  7.61 us (5%)
  local copies, waits for them, and re-layouts  4.46 us (3%)
  other arithmetic  1.88 us (1%)
    all_gather x1, waiting for transfers between devices, per_device(): lax.all_gather(out_conv, 'sp', axis=1, tiled=True)  47.5 us
    reduce_scatter x1, waiting for transfers between devices, per_device(): lax.psum_scatter((summed + jnp.dot(conv_mix, wide_conv, preferred_element...  23.1 us
    all_gather x1, blocking collectives, per_device(): decays = lax.all_gather(device_decay[None], 'sp', axis=0, tiled=True)  21.3 us
    all_gather x1, waiting for transfers between devices, per_device(): lax.all_gather(out_gla, 'sp', axis=1, tiled=True)  8.57 us
    all_to_all x1, starting transfers between devices, per_device(): lax.all_to_all(device_state[None].astype(jnp.bfloat16), 'sp', split_axis=...  7.28 us
    all_to_all x1, waiting for transfers between devices, per_device(): lax.all_to_all(for_sending(before), 'sp', split_axis=0, concat_axis=3, ti...  5.2 us
    ppermute x1, starting transfers between devices, from_behind(): return lax.ppermute(x, axis, pairs)  3.77 us
    dot_general x1, matrix products, per_device(): jnp.dot(conv_mix, wide_conv, preferred_element_type=jnp.float32)  3.39 us
  transfers between devices with their start and end apart: 6, of which 4 were waited for; matrix products, arithmetic and copies ran while one was open for 7% of the time, Pallas kernels for 0%

commit v1 on v0

--- a/solution.py
+++ b/solution.py
@@ -1,6 +1,10 @@
+import functools
+
 import jax
 import jax.numpy as jnp
 from jax import lax
+from jax.experimental import pallas as pl
+from jax.experimental.pallas import tpu as pltpu
 from jax.sharding import PartitionSpec as P
 
 KEY_WIDTH = 128
@@ -103,6 +107,344 @@
     )
 
 
+MESH = pl.DeviceIdType.MESH
+LANES = 128
+HALO = 16
+CHUNKS = 2
+SPLIT = 2
+BITS = 3
+
+
+def flipped(index, bit):
+    return index + bit - 2 * bit * ((index // bit) % 2)
+
+
+def fits(mesh):
+    return mesh.shape["sp"] == SPLIT**BITS
+
+
+def kernel(
+    n_sp,
+    n_tp,
+    q_ref,
+    k_ref,
+    v_ref,
+    code_ref,
+    up_ref,
+    bias_ref,
+    gain_ref,
+    x_ref,
+    cg_ref,
+    taps_ref,
+    wg_ref,
+    wc_ref,
+    out_ref,
+    halo,
+    ext,
+    st,
+    dec,
+    cols,
+    bef,
+    inc,
+    sloc,
+    thr,
+    mix,
+    wbuf,
+    cbuf,
+    crecv,
+    halo_sem,
+    a_sem,
+    d_sem,
+    b_sem,
+    w_sem,
+    mix_sem,
+    c_sem,
+):
+    s, t = lax.axis_index("sp"), lax.axis_index("tp")
+    f32, bf16 = jnp.float32, jnp.bfloat16
+    rows, key_cols = q_ref.shape
+    seg = SEGMENT_LENGTH
+    segs = rows // seg
+    heads = key_cols // KEY_WIDTH
+    val_rows = HEAD_V // n_sp
+    chan, width = wg_ref.shape
+    piece = rows // n_tp
+    started = []
+
+    def send(src, dst, sems, where):
+        copy = pltpu.make_async_remote_copy(
+            src_ref=src,
+            dst_ref=dst,
+            send_sem=sems[0],
+            recv_sem=sems[1],
+            device_id=where,
+            device_id_type=MESH,
+        )
+        copy.start()
+        started.append(copy)
+        return copy
+
+    def pair(sem, *index):
+        return sem.at[(0, *index)], sem.at[(1, *index)]
+
+    side, low, far = flipped(s, 1), flipped(s, 2), flipped(s, 4)
+
+    barrier = pltpu.get_barrier_semaphore()
+    greet = [(lax.rem(s + d, n_sp), t) for d in range(1, n_sp)]
+    greet += [(p, lax.rem(t + d, n_tp)) for p in (s, low) for d in range(1, n_tp)]
+    for where in greet:
+        pl.semaphore_signal(barrier, inc=1, device_id=where, device_id_type=MESH)
+    pl.semaphore_wait(barrier, len(greet))
+
+    halo_copy = send(
+        x_ref.at[pl.ds(rows - HALO, HALO)], halo, pair(halo_sem), (lax.rem(s + 1, n_sp), t)
+    )
+
+    weight = (wc_ref, wg_ref)
+    step = chan // CHUNKS
+    to_side, to_far, onward = {}, {}, {}
+
+    def send_chunk(half, c):
+        part = pl.ds(c * step, step)
+        to_far[half, c] = send(
+            weight[half].at[part], wbuf.at[half, 1, part], pair(w_sem, 1, half, c), (far, t)
+        )
+        to_side[half, c] = send(
+            weight[half].at[part], wbuf.at[half, 0, part], pair(w_sem, 0, half, c), (side, t)
+        )
+
+    def pass_on(half, c):
+        part = pl.ds(c * step, step)
+        to_far[half, c].wait_recv()
+        onward[half, c] = send(
+            wbuf.at[half, 1, part], wbuf.at[half, 2, part], pair(w_sem, 2, half, c), (side, t)
+        )
+
+    send_chunk(0, 0)
+
+    g = jnp.dot(code_ref[...], up_ref[...], preferred_element_type=f32) + bias_ref[...]
+    log_decay = (jnp.minimum(g, 0.0) - jnp.log1p(jnp.exp(-jnp.abs(g)))) / softness_divisor
+    row_i = lax.broadcasted_iota(jnp.int32, (seg, seg), 0)
+    col_i = lax.broadcasted_iota(jnp.int32, (seg, seg), 1)
+    later = (col_i > row_i).astype(f32)
+    state = None
+    passed = None
+    for n in range(segs):
+        here = pl.ds(n * seg, seg)
+        block = log_decay[n * seg : (n + 1) * seg]
+        rest = jnp.dot(
+            later, block, preferred_element_type=f32, precision=lax.Precision.HIGHEST
+        )
+        total = jnp.sum(block, axis=0, keepdims=True)
+        scaled = (k_ref[here, :].astype(f32) * jnp.exp(rest)).astype(bf16)
+        update = jnp.concatenate(
+            [
+                lax.dot_general(
+                    v_ref[here, pl.ds(h * HEAD_V, HEAD_V)],
+                    scaled[:, h * KEY_WIDTH : (h + 1) * KEY_WIDTH],
+                    (((0,), (0,)), ((), ())),
+                    preferred_element_type=f32,
+                )
+                for h in range(heads)
+            ],
+            axis=1,
+        )
+        if n == 0:
+            state, passed = update, total
+        else:
+            state, passed = jnp.exp(total) * state + update, passed + total
+        sloc[n] = state
+        thr[n] = jnp.exp(passed)
+    st[...] = state.astype(bf16).reshape(st.shape)
+    dec[s] = jnp.exp(passed)
+    cols[s] = st[s]
+
+    first = []
+    for d in range(1, n_sp):
+        dst = lax.rem(s + d, n_sp)
+        first.append(send(st.at[dst], cols.at[s], pair(a_sem, d - 1), (dst, t)))
+        first.append(send(dec.at[s], dec.at[s], pair(d_sem, d - 1), (dst, t)))
+
+    send_chunk(0, 1)
+
+    halo_copy.wait_recv()
+    ext[pl.ds(0, HALO), :] = jnp.where(s > 0, halo[...].astype(f32), 0.0)
+    ext[pl.ds(HALO, rows), :] = x_ref[...].astype(f32)
+    taps = taps_ref.shape[0]
+    total = None
+    for o in range(taps):
+        term = taps_ref[pl.ds(o, 1), :] * ext[pl.ds(HALO - taps + 1 + o, rows), :]
+        total = term if total is None else total + term
+    mix[0, 0] = (cg_ref[...].astype(f32) * total).astype(bf16)
+
+    for copy in first:
+        copy.wait_recv()
+    running = jnp.zeros(cols.shape[1:], f32)
+    for j in range(n_sp):
+        bef[j] = running.astype(bf16)
+        if j < n_sp - 1:
+            running = dec[j] * running + cols[j].astype(f32)
+    inc[s] = bef[s]
+    second = []
+    for d in range(1, n_sp):
+        dst = lax.rem(s + d, n_sp)
+        second.append(send(bef.at[dst], inc.at[s], pair(b_sem, d - 1), (dst, t)))
+
+    mix_copies = {0: send(mix.at[0, 0], mix.at[1, 0], pair(mix_sem, 0), (low, t))}
+    send_chunk(1, 0)
+    pass_on(0, 0)
+
+    for copy in second:
+        copy.wait_recv()
+    incoming = inc[...].astype(f32).reshape(HEAD_V, key_cols)
+    for n in range(segs):
+        here = pl.ds(n * seg, seg)
+        full = (sloc[n] + thr[n] * incoming).astype(bf16)
+        for h in range(heads):
+            lanes = slice(h * KEY_WIDTH, (h + 1) * KEY_WIDTH)
+            read = lax.dot_general(
+                q_ref[here, lanes],
+                full[:, lanes],
+                (((1,), (1,)), ((), ())),
+                preferred_element_type=f32,
+            )
+            scale = lax.rsqrt(jnp.mean(read * read, axis=-1, keepdims=True) + epsilon)
+            mix[0, 1, here, pl.ds(h * HEAD_V, HEAD_V)] = (
+                read * scale * gain_ref[...]
+            ).astype(bf16)
+    mix_copies[1] = send(mix.at[0, 1], mix.at[1, 1], pair(mix_sem, 1), (low, t))
+    for c in range(1, CHUNKS):
+        send_chunk(1, c)
+        pass_on(0, c)
+
+    results = {}
+
+    def product(whose, slot):
+        acc = None
+        for half in range(2):
+            w = weight[half][...] if slot == 0 else wbuf[half, slot - 1]
+            term = jnp.dot(mix[whose, half], w, preferred_element_type=f32)
+            acc = term if acc is None else acc + term
+        cbuf[whose, slot] = acc.astype(bf16)
+        for d in range(n_tp - 1, -1, -1):
+            if whose == 0 and d == 0:
+                continue
+            other = lax.rem(t + d, n_tp)
+            part = pl.ds(pl.multiple_of(other * piece, piece), piece)
+            results[whose, d, slot] = send(
+                cbuf.at[whose, slot, part],
+                crecv.at[whose, d, slot],
+                pair(c_sem, whose, d, slot),
+                (low if whose else s, other),
+            )
+
+    product(0, 0)
+    for half in range(2):
+        for c in range(CHUNKS):
+            to_side[half, c].wait_recv()
+    product(0, 1)
+    for c in range(CHUNKS):
+        pass_on(1, c)
+    for half in range(2):
+        mix_copies[half].wait_recv()
+    product(1, 0)
+    product(1, 1)
+    product(1, 2)
+    product(0, 2)
+    for half in range(2):
+        for c in range(CHUNKS):
+            onward[half, c].wait_recv()
+    product(1, 3)
+    product(0, 3)
+
+    mine = pl.ds(pl.multiple_of(t * piece, piece), piece)
+    for slot in range(4):
+        for whose in range(2):
+            total = cbuf[0, slot, mine, :].astype(f32) if whose == 0 else None
+            for d in range(n_tp):
+                if whose == 0 and d == 0:
+                    continue
+                results[whose, d, slot].wait_recv()
+                term = crecv[whose, d, slot].astype(f32)
+                total = term if total is None else total + term
+            block = low if whose else s
+            if slot % 2:
+                block = flipped(block, 1)
+            if slot // 2:
+                block = flipped(block, 4)
+            place = pl.ds(pl.multiple_of(block * width, width), width)
+            out_ref[:, place] = total.astype(bf16)
+    for copy in started:
+        copy.wait_send()
+
+
+def fused(
+    queries,
+    keys,
+    values,
+    gate_code,
+    gate_up,
+    gate_bias,
+    gla_gain,
+    conv_input,
+    conv_gate,
+    conv_taps,
+    out_gla,
+    out_conv,
+):
+    n_sp, n_tp = lax.axis_size("sp"), lax.axis_size("tp")
+    rows, key_cols = queries.shape
+    segs = rows // SEGMENT_LENGTH
+    chan, width = out_gla.shape
+    bf16, f32 = jnp.bfloat16, jnp.float32
+    val_rows = HEAD_V // n_sp
+    dma = pltpu.SemaphoreType.DMA
+    return pl.pallas_call(
+        functools.partial(kernel, n_sp, n_tp),
+        out_shape=jax.ShapeDtypeStruct((rows // n_tp, n_sp * width), bf16),
+        in_specs=[pl.BlockSpec(memory_space=pltpu.VMEM)] * 12,
+        out_specs=pl.BlockSpec(memory_space=pltpu.VMEM),
+        scratch_shapes=[
+            pltpu.VMEM((HALO, conv_input.shape[1]), bf16),
+            pltpu.VMEM((HALO + rows, conv_input.shape[1]), f32),
+            pltpu.VMEM((n_sp, val_rows, key_cols), bf16),
+            pltpu.VMEM((n_sp, 1, key_cols), f32),
+            pltpu.VMEM((n_sp, val_rows, key_cols), bf16),
+            pltpu.VMEM((n_sp, val_rows, key_cols), bf16),
+            pltpu.VMEM((n_sp, val_rows, key_cols), bf16),
+            pltpu.VMEM((segs, HEAD_V, key_cols), f32),
+            pltpu.VMEM((segs, 1, key_cols), f32),
+            pltpu.VMEM((2, 2, rows, chan), bf16),
+            pltpu.VMEM((2, 3, chan, width), bf16),
+            pltpu.VMEM((2, 4, rows, width), bf16),
+            pltpu.VMEM((2, n_tp, 4, rows // n_tp, width), bf16),
+            dma((2,)),
+            dma((2, n_sp - 1)),
+            dma((2, n_sp - 1)),
+            dma((2, n_sp - 1)),
+            dma((2, 3, 2, CHUNKS)),
+            dma((2, 2)),
+            dma((2, 2, n_tp, 4)),
+        ],
+        compiler_params=pltpu.CompilerParams(
+            collective_id=0, has_side_effects=True, vmem_limit_bytes=48 * 1024 * 1024
+        ),
+    )(
+        queries,
+        keys,
+        values,
+        gate_code,
+        gate_up,
+        gate_bias[None],
+        gla_gain[None],
+        conv_input,
+        conv_gate,
+        conv_taps,
+        out_gla,
+        out_conv,
+    )
+
+
 def solution(mesh):
     in_specs = (
         P("sp", "tp"),
@@ -120,5 +462,5 @@
     )
     out_specs = P(("sp", "tp"), None)
     return jax.shard_map(
-        per_device, mesh=mesh, in_specs=in_specs, out_specs=out_specs, check_vma=False
-    )
+        fused if fits(mesh) else per_device, mesh=mesh, in_specs=in_specs, out_specs=out_specs, check_vma=False
+    )

time: 150 us -> 63 us (0.42)
  waiting for transfers between devices: 85.9 us -> 0 us
  Pallas kernels: 0 us -> 54.4 us
  blocking collectives: 21.3 us -> 0 us
  starting transfers between devices: 14.5 us -> 0 us
  between operations: 13.7 us -> 0.06 us
  matrix products: 7.61 us -> 0 us
  local copies, waits for them, and re-layouts: 4.46 us -> 8.16 us
  other arithmetic: 1.88 us -> 0 us
    all_gather x2 -> x0, waiting for transfers between devices: 56.1 us -> none  [the longest x1 47.5 us: per_device(): lax.all_gather(out_conv, 'sp', axis=1, tiled=True)]
    pallas_call x0 -> x1, Pallas kernels: none -> 54.4 us  [fused(): pl.pallas_call(functools.partial(kernel, n_sp, n_tp), out_shape=jax.Shape...]
    reduce_scatter x1 -> x0, waiting for transfers between devices: 23.1 us -> none  [per_device(): lax.psum_scatter((summed + jnp.dot(conv_mix, wide_conv, preferred_element...]
    all_gather x1 -> x0, blocking collectives: 21.3 us -> none  [per_device(): decays = lax.all_gather(device_decay[None], 'sp', axis=0, tiled=True)]
    all_to_all x2 -> x0, starting transfers between devices: 10.7 us -> none  [the longest x1 7.28 us: per_device(): lax.all_to_all(device_state[None].astype(jnp.bfloat16), 'sp', split_axis=...]
    unnamed x25 -> x24, local copies, waits for them, and re-layouts: 0.19 us -> 8.16 us
    dot_general x5 -> x0, matrix products: 7.61 us -> none  [the longest x1 3.39 us: per_device(): jnp.dot(conv_mix, wide_conv, preferred_element_type=jnp.float32)]
    all_to_all x2 -> x0, waiting for transfers between devices: 5.2 us -> none  [the longest x1 5.2 us: per_device(): lax.all_to_all(for_sending(before), 'sp', split_axis=0, concat_axis=3, ti...]
  transfers between devices with their start and end apart: 6 -> 0, of which waited for: 4 -> 0; matrix products, arithmetic and copies ran while one was open for 7% -> 0% of each run, Pallas kernels for 0% -> 0%
where the time goes in v1:
time: 63 us; the launch traced here: 62.6 us
  Pallas kernels  54.4 us (86%)
  local copies, waits for them, and re-layouts  8.16 us (13%)
    pallas_call x1, Pallas kernels, fused(): pl.pallas_call(functools.partial(kernel, n_sp, n_tp), out_shape=jax.Shape...  54.4 us
    unnamed x24, local copies, waits for them, and re-layouts  8.16 us

profile of v1, /device:TPU:0, one launch (start us, length us, event | category | flops | bytes accessed | tf_op | source)
XLA Modules:
  0.0 62.6 jit_solution(2039782774757591554)
XLA Ops:
  0.0 0.0 copy-start.7
  0.0 0.0 copy-start.8
  0.0 0.0 copy-start.9
  0.0 0.0 copy-start.10
  0.0 0.9 %copy.13.code_ref = bf16[256,32]{1,0:T(8,128)(2,1)S(1)} copy(bf16[256,32]{0,1:T(8,128)(2,1)} %param.15) | data formatting | bytes 32768 | tf_op args[3]
  0.9 0.0 copy-done.7
  0.9 0.0 copy-done.8
  0.9 0.0 copy-done.9
  0.9 0.0 copy-done.10
  0.9 0.0 copy-start
  0.9 0.9 %copy-done = bf16[256,512]{1,0:T(8,128)(2,1)S(1)} copy-done((bf16[256,512]{1,0:T(8,128)(2,1)S(1)}, bf16[256,512]{1,0:T(8,128)(2,1)}, u32[]{:S(2)}) %copy-start) | copy-done | bytes 262168
  1.9 0.0 copy-start.1
  1.9 0.9 %copy-done.1 = bf16[256,512]{1,0:T(8,128)(2,1)S(1)} copy-done((bf16[256,512]{1,0:T(8,128)(2,1)S(1)}, bf16[256,512]{1,0:T(8,128)(2,1)}, u32[]{:S(2)}) %copy-start.1) | copy-done | bytes 262168
  2.8 0.0 copy-start.2
  2.8 0.9 %copy-done.2 = bf16[256,512]{1,0:T(8,128)(2,1)S(1)} copy-done((bf16[256,512]{1,0:T(8,128)(2,1)S(1)}, bf16[256,512]{1,0:T(8,128)(2,1)}, u32[]{:S(2)}) %copy-start.2) | copy-done | bytes 262168
  3.8 0.0 copy-start.3
  3.8 0.9 %copy-done.3 = bf16[512,256]{1,0:T(8,128)(2,1)S(1)} copy-done((bf16[512,256]{1,0:T(8,128)(2,1)S(1)}, bf16[512,256]{1,0:T(8,128)(2,1)}, u32[]{:S(2)}) %copy-start.3) | copy-done | bytes 262168
  4.7 0.0 copy-start.4
  4.7 0.9 %copy-done.4 = bf16[512,256]{1,0:T(8,128)(2,1)S(1)} copy-done((bf16[512,256]{1,0:T(8,128)(2,1)S(1)}, bf16[512,256]{1,0:T(8,128)(2,1)}, u32[]{:S(2)}) %copy-start.4) | copy-done | bytes 262168
  5.7 0.0 copy-start.5
  5.7 0.9 %copy-done.5 = bf16[256,256]{1,0:T(8,128)(2,1)S(1)} copy-done((bf16[256,256]{1,0:T(8,128)(2,1)S(1)}, bf16[256,256]{1,0:T(8,128)(2,1)}, u32[]{:S(2)}) %copy-start.5) | copy-done | bytes 131096
  6.6 0.0 copy-start.6
  6.6 0.9 %copy-done.6 = bf16[256,256]{1,0:T(8,128)(2,1)S(1)} copy-done((bf16[256,256]{1,0:T(8,128)(2,1)S(1)}, bf16[256,256]{1,0:T(8,128)(2,1)}, u32[]{:S(2)}) %copy-start.6) | copy-done | bytes 131096
  7.5 54.4 %shard_map.118 = bf16[64,2048]{1,0:T(8,128)(2,1)S(1)} custom-call(bf16[256,256]{1,0:T(8,128)(2,1)S(1)} %copy-done.5, bf16[256,256]{1,0:T(8,128)(2,1)S(1)} %copy-done.6, bf16[256,512]{1,0:T(8,128)(2,1)S(1)} %copy-done, bf16[256,32]{1,0:T(8,128)(2,1)S(1)} %copy.13.code_ref, bf16[32,256]{1,0:T(8,128)(2,1)S(1)} %copy-done.7, f32[1,256]{1,0:T(1,128)S(1)} %bitcast.2, ...), custom_call_target="tpu_custom_call" | custom-call | tf_op jit(solution)/shard_map/pallas_call | solution.py:402
  61.9 0.7 %copy.15 = bf16[64,2048]{1,0:T(8,128)(2,1)} copy(bf16[64,2048]{1,0:T(8,128)(2,1)S(1)} %shard_map.118) | data formatting | bytes 524288
Async XLA Ops:
  0.0 0.9 %copy-start.7 = (bf16[32,256]{1,0:T(8,128)(2,1)S(1)}, bf16[32,256]{1,0:T(8,128)(2,1)}, u32[]{:S(2)}) copy-start(bf16[32,256]{1,0:T(8,128)(2,1)} %up_ref.1) | copy-start | bytes 49156
  0.0 0.9 %copy-start.8 = (f32[3,512]{1,0:T(4,128)S(1)}, f32[3,512]{1,0:T(4,128)}, u32[]{:S(2)}) copy-start(f32[3,512]{1,0:T(4,128)} %taps_ref.1) | copy-start | bytes 18436
  0.0 0.9 %copy-start.9 = (f32[256]{0:T(256)S(1)}, f32[256]{0:T(256)}, u32[]{:S(2)}) copy-start(f32[256]{0:T(256)} %param.17) | copy-start | bytes 3076
  0.0 0.9 %copy-start.10 = (f32[256]{0:T(256)S(1)}, f32[256]{0:T(256)}, u32[]{:S(2)}) copy-start(f32[256]{0:T(256)} %param.18) | copy-start | bytes 3076
  0.9 1.0 %copy-start = (bf16[256,512]{1,0:T(8,128)(2,1)S(1)}, bf16[256,512]{1,0:T(8,128)(2,1)}, u32[]{:S(2)}) copy-start(bf16[256,512]{1,0:T(8,128)(2,1)} %v_ref.1) | copy-start | bytes 786436
  1.9 0.9 %copy-start.1 = (bf16[256,512]{1,0:T(8,128)(2,1)S(1)}, bf16[256,512]{1,0:T(8,128)(2,1)}, u32[]{:S(2)}) copy-start(bf16[256,512]{1,0:T(8,128)(2,1)} %x_ref.1) | copy-start | bytes 786436
  2.8 0.9 %copy-start.2 = (bf16[256,512]{1,0:T(8,128)(2,1)S(1)}, bf16[256,512]{1,0:T(8,128)(2,1)}, u32[]{:S(2)}) copy-start(bf16[256,512]{1,0:T(8,128)(2,1)} %cg_ref.1) | copy-start | bytes 786436
  3.8 0.9 %copy-start.3 = (bf16[512,256]{1,0:T(8,128)(2,1)S(1)}, bf16[512,256]{1,0:T(8,128)(2,1)}, u32[]{:S(2)}) copy-start(bf16[512,256]{1,0:T(8,128)(2,1)} %wg_ref.1) | copy-start | bytes 786436
  4.7 0.9 %copy-start.4 = (bf16[512,256]{1,0:T(8,128)(2,1)S(1)}, bf16[512,256]{1,0:T(8,128)(2,1)}, u32[]{:S(2)}) copy-start(bf16[512,256]{1,0:T(8,128)(2,1)} %wc_ref.1) | copy-start | bytes 786436
  5.7 0.9 %copy-start.5 = (bf16[256,256]{1,0:T(8,128)(2,1)S(1)}, bf16[256,256]{1,0:T(8,128)(2,1)}, u32[]{:S(2)}) copy-start(bf16[256,256]{1,0:T(8,128)(2,1)} %q_ref.1) | copy-start | bytes 393220
  6.6 0.9 %copy-start.6 = (bf16[256,256]{1,0:T(8,128)(2,1)S(1)}, bf16[256,256]{1,0:T(8,128)(2,1)}, u32[]{:S(2)}) copy-start(bf16[256,256]{1,0:T(8,128)(2,1)} %k_ref.1) | copy-start | bytes 393220

commit v2 on v1

--- a/solution.py
+++ b/solution.py
@@ -108,6 +108,7 @@
 
 
 MESH = pl.DeviceIdType.MESH
+ARGS = 12
 LANES = 128
 HALO = 16
 CHUNKS = 2
@@ -120,25 +121,26 @@
 
 
 def fits(mesh):
-    return mesh.shape["sp"] == SPLIT**BITS
+    return mesh.shape["sp"] == SPLIT**BITS and mesh.shape["tp"] == SPLIT**2
 
 
 def kernel(
     n_sp,
     n_tp,
-    q_ref,
-    k_ref,
-    v_ref,
-    code_ref,
-    up_ref,
-    bias_ref,
-    gain_ref,
-    x_ref,
-    cg_ref,
-    taps_ref,
-    wg_ref,
-    wc_ref,
+    *refs,
+):
+    sources, out_ref, scratch = refs[:ARGS], refs[ARGS], refs[ARGS + 1 :]
+    held, scratch = scratch[:ARGS], scratch[ARGS:]
+    body(n_sp, n_tp, sources, held, out_ref, *scratch)
+
+
+def body(
+    n_sp,
+    n_tp,
+    sources,
+    held,
     out_ref,
+    in_sem,
     halo,
     ext,
     st,
@@ -151,6 +153,8 @@
     mix,
     wbuf,
     cbuf,
+    mrecv,
+    csum,
     crecv,
     halo_sem,
     a_sem,
@@ -158,8 +162,33 @@
     b_sem,
     w_sem,
     mix_sem,
+    m_sem,
     c_sem,
 ):
+    (
+        q_ref,
+        k_ref,
+        v_ref,
+        code_ref,
+        up_ref,
+        bias_ref,
+        gain_ref,
+        x_ref,
+        cg_ref,
+        taps_ref,
+        wg_ref,
+        wc_ref,
+    ) = held
+    loads = [pltpu.make_async_copy(a, b, in_sem.at[i]) for i, (a, b) in enumerate(zip(sources, held))]
+    loading = list(range(ARGS))
+
+    def need(*which):
+        for i in which:
+            loads[i].wait()
+            loading.remove(i)
+
+    for i in (7, 11, 3, 4, 5, 1, 2, 10, 8, 9, 0, 6):
+        loads[i].start()
     s, t = lax.axis_index("sp"), lax.axis_index("tp")
     f32, bf16 = jnp.float32, jnp.bfloat16
     rows, key_cols = q_ref.shape
@@ -191,11 +220,13 @@
 
     barrier = pltpu.get_barrier_semaphore()
     greet = [(lax.rem(s + d, n_sp), t) for d in range(1, n_sp)]
-    greet += [(p, lax.rem(t + d, n_tp)) for p in (s, low) for d in range(1, n_tp)]
+    mate, across = flipped(t, 1), flipped(t, 2)
+    greet += [(s, mate), (s, across), (low, across)]
     for where in greet:
         pl.semaphore_signal(barrier, inc=1, device_id=where, device_id_type=MESH)
     pl.semaphore_wait(barrier, len(greet))
 
+    need(7, 11)
     halo_copy = send(
         x_ref.at[pl.ds(rows - HALO, HALO)], halo, pair(halo_sem), (lax.rem(s + 1, n_sp), t)
     )
@@ -222,7 +253,16 @@
 
     send_chunk(0, 0)
 
-    g = jnp.dot(code_ref[...], up_ref[...], preferred_element_type=f32) + bias_ref[...]
+    need(3, 4, 5, 1, 2)
+    g = (
+        lax.dot_general(
+            code_ref[...],
+            up_ref[...],
+            (((0,), (0,)), ((), ())),
+            preferred_element_type=f32,
+        )
+        + bias_ref[...]
+    )
     log_decay = (jnp.minimum(g, 0.0) - jnp.log1p(jnp.exp(-jnp.abs(g)))) / softness_divisor
     row_i = lax.broadcasted_iota(jnp.int32, (seg, seg), 0)
     col_i = lax.broadcasted_iota(jnp.int32, (seg, seg), 1)
@@ -268,6 +308,7 @@
     send_chunk(0, 1)
 
     halo_copy.wait_recv()
+    need(8, 9)
     ext[pl.ds(0, HALO), :] = jnp.where(s > 0, halo[...].astype(f32), 0.0)
     ext[pl.ds(HALO, rows), :] = x_ref[...].astype(f32)
     taps = taps_ref.shape[0]
@@ -290,8 +331,10 @@
         dst = lax.rem(s + d, n_sp)
         second.append(send(bef.at[dst], inc.at[s], pair(b_sem, d - 1), (dst, t)))
 
+    need(10, 0, 6)
+    for c in range(CHUNKS):
+        send_chunk(1, c)
     mix_copies = {0: send(mix.at[0, 0], mix.at[1, 0], pair(mix_sem, 0), (low, t))}
-    send_chunk(1, 0)
     pass_on(0, 0)
 
     for copy in second:
@@ -314,10 +357,12 @@
             ).astype(bf16)
     mix_copies[1] = send(mix.at[0, 1], mix.at[1, 1], pair(mix_sem, 1), (low, t))
     for c in range(1, CHUNKS):
-        send_chunk(1, c)
         pass_on(0, c)
 
-    results = {}
+    halves, results = {}, {}
+
+    def rows_of(owner):
+        return pl.ds(pl.multiple_of(owner * piece, piece), piece)
 
     def product(whose, slot):
         acc = None
@@ -326,47 +371,67 @@
             term = jnp.dot(mix[whose, half], w, preferred_element_type=f32)
             acc = term if acc is None else acc + term
         cbuf[whose, slot] = acc.astype(bf16)
-        for d in range(n_tp - 1, -1, -1):
-            if whose == 0 and d == 0:
-                continue
-            other = lax.rem(t + d, n_tp)
-            part = pl.ds(pl.multiple_of(other * piece, piece), piece)
-            results[whose, d, slot] = send(
-                cbuf.at[whose, slot, part],
-                crecv.at[whose, d, slot],
-                pair(c_sem, whose, d, slot),
-                (low if whose else s, other),
+        for dy in (1, 0):
+            owner = flipped(across, 1) if dy else mate
+            halves[whose, slot, dy] = send(
+                cbuf.at[whose, slot, rows_of(owner)],
+                mrecv.at[whose, slot, dy],
+                pair(m_sem, whose, slot, dy),
+                (s, mate),
             )
+
+    def finish(whose, slot):
+        for dy in (1, 0):
+            owner = across if dy else t
+            halves[whose, slot, dy].wait_recv()
+            both = cbuf[whose, slot, rows_of(owner), :].astype(f32) + mrecv[
+                whose, slot, dy
+            ].astype(f32)
+            csum[whose, slot, dy] = both.astype(bf16)
+            if whose or dy:
+                results[whose, slot, dy] = send(
+                    csum.at[whose, slot, dy],
+                    crecv.at[whose, slot, dy],
+                    pair(c_sem, whose, slot, dy),
+                    (low if whose else s, owner),
+                )
 
     product(0, 0)
     for half in range(2):
         for c in range(CHUNKS):
             to_side[half, c].wait_recv()
     product(0, 1)
-    for c in range(CHUNKS):
-        pass_on(1, c)
+    finish(0, 0)
+    finish(0, 1)
     for half in range(2):
         mix_copies[half].wait_recv()
     product(1, 0)
     product(1, 1)
+    finish(1, 0)
+    finish(1, 1)
+    for c in range(CHUNKS):
+        pass_on(1, c)
     product(1, 2)
     product(0, 2)
+    finish(1, 2)
+    finish(0, 2)
     for half in range(2):
         for c in range(CHUNKS):
             onward[half, c].wait_recv()
     product(1, 3)
     product(0, 3)
-
-    mine = pl.ds(pl.multiple_of(t * piece, piece), piece)
+    finish(1, 3)
+    finish(0, 3)
+
     for slot in range(4):
         for whose in range(2):
-            total = cbuf[0, slot, mine, :].astype(f32) if whose == 0 else None
-            for d in range(n_tp):
-                if whose == 0 and d == 0:
-                    continue
-                results[whose, d, slot].wait_recv()
-                term = crecv[whose, d, slot].astype(f32)
-                total = term if total is None else total + term
+            results[whose, slot, 1].wait_recv()
+            if whose:
+                results[1, slot, 0].wait_recv()
+                total = crecv[1, slot, 0].astype(f32)
+            else:
+                total = csum[0, slot, 0].astype(f32)
+            total = total + crecv[whose, slot, 1].astype(f32)
             block = low if whose else s
             if slot % 2:
                 block = flipped(block, 1)
@@ -399,12 +464,28 @@
     bf16, f32 = jnp.bfloat16, jnp.float32
     val_rows = HEAD_V // n_sp
     dma = pltpu.SemaphoreType.DMA
+    operands = (
+        queries,
+        keys,
+        values,
+        gate_code.T,
+        gate_up,
+        gate_bias[None],
+        gla_gain[None],
+        conv_input,
+        conv_gate,
+        conv_taps,
+        out_gla,
+        out_conv,
+    )
     return pl.pallas_call(
         functools.partial(kernel, n_sp, n_tp),
         out_shape=jax.ShapeDtypeStruct((rows // n_tp, n_sp * width), bf16),
-        in_specs=[pl.BlockSpec(memory_space=pltpu.VMEM)] * 12,
+        in_specs=[pl.BlockSpec(memory_space=pltpu.HBM)] * ARGS,
         out_specs=pl.BlockSpec(memory_space=pltpu.VMEM),
         scratch_shapes=[
+            *(pltpu.VMEM(a.shape, a.dtype) for a in operands),
+            dma((ARGS,)),
             pltpu.VMEM((HALO, conv_input.shape[1]), bf16),
             pltpu.VMEM((HALO + rows, conv_input.shape[1]), f32),
             pltpu.VMEM((n_sp, val_rows, key_cols), bf16),
@@ -417,32 +498,22 @@
             pltpu.VMEM((2, 2, rows, chan), bf16),
             pltpu.VMEM((2, 3, chan, width), bf16),
             pltpu.VMEM((2, 4, rows, width), bf16),
-            pltpu.VMEM((2, n_tp, 4, rows // n_tp, width), bf16),
+            pltpu.VMEM((2, 4, 2, rows // n_tp, width), bf16),
+            pltpu.VMEM((2, 4, 2, rows // n_tp, width), bf16),
+            pltpu.VMEM((2, 4, 2, rows // n_tp, width), bf16),
             dma((2,)),
             dma((2, n_sp - 1)),
             dma((2, n_sp - 1)),
             dma((2, n_sp - 1)),
             dma((2, 3, 2, CHUNKS)),
             dma((2, 2)),
-            dma((2, 2, n_tp, 4)),
+            dma((2, 2, 4, 2)),
+            dma((2, 2, 4, 2)),
         ],
         compiler_params=pltpu.CompilerParams(
-            collective_id=0, has_side_effects=True, vmem_limit_bytes=48 * 1024 * 1024
+            collective_id=0, has_side_effects=True, vmem_limit_bytes=67043328
         ),
-    )(
-        queries,
-        keys,
-        values,
-        gate_code,
-        gate_up,
-        gate_bias[None],
-        gla_gain[None],
-        conv_input,
-        conv_gate,
-        conv_taps,
-        out_gla,
-        out_conv,
-    )
+    )(*operands)
 
 
 def solution(mesh):

time: 63 us -> 58.6 us (0.930)
  local copies, waits for them, and re-layouts: 8.16 us -> 1.67 us
  Pallas kernels: 54.4 us -> 56.7 us
    unnamed x24 -> x1, local copies, waits for them, and re-layouts: 8.16 us -> 1.67 us
    pallas_call x1, Pallas kernels: 54.4 us -> 56.7 us  [fused(): pl.pallas_call(functools.partial(kernel, n_sp, n_tp), out_shape=jax.Shape...]
where the time goes in v2:
time: 58.6 us; the launch traced here: 58.4 us
  Pallas kernels  56.7 us (97%)
  local copies, waits for them, and re-layouts  1.67 us (3%)
    pallas_call x1, Pallas kernels, fused(): pl.pallas_call(functools.partial(kernel, n_sp, n_tp), out_shape=jax.Shape...  56.7 us
    unnamed x1, local copies, waits for them, and re-layouts  1.67 us

profile of v2, /device:TPU:0, one launch (start us, length us, event | category | flops | bytes accessed | tf_op | source)
XLA Modules:
  0.0 58.4 jit_solution(5466228620657998412)
XLA Ops:
  0.0 56.7 %shard_map.118 = bf16[64,2048]{1,0:T(8,128)(2,1)} custom-call(bf16[256,256]{1,0:T(8,128)(2,1)} %refs_0_.1, bf16[256,256]{1,0:T(8,128)(2,1)} %refs_1_.1, bf16[256,512]{1,0:T(8,128)(2,1)} %refs_2_.1, bf16[32,256]{1,0:T(8,128)(2,1)} %bitcast.3, bf16[32,256]{1,0:T(8,128)(2,1)} %refs_4_.1, f32[1,256]{1,0:T(1,128)} %bitcast.4, f32[1,256]{1,0:T(1,128)} %bitcast.5, ...), custom_call_target="tpu_custom_call" | custom-call | tf_op jit(solution)/shard_map/pallas_call | solution.py:481
  56.7 1.7 %copy.14 = bf16[64,2048]{1,0:T(8,128)(2,1)} copy(bf16[64,2048]{1,0:T(8,128)(2,1)} %shard_map.118) | data formatting | bytes 524288

commit v3 on v2

--- a/solution.py
+++ b/solution.py
@@ -224,25 +224,44 @@
     greet += [(s, mate), (s, across), (low, across)]
     for where in greet:
         pl.semaphore_signal(barrier, inc=1, device_id=where, device_id_type=MESH)
-    pl.semaphore_wait(barrier, len(greet))
-
-    need(7, 11)
-    halo_copy = send(
-        x_ref.at[pl.ds(rows - HALO, HALO)], halo, pair(halo_sem), (lax.rem(s + 1, n_sp), t)
-    )
 
     weight = (wc_ref, wg_ref)
     step = chan // CHUNKS
     to_side, to_far, onward = {}, {}, {}
 
-    def send_chunk(half, c):
+    def over_side(half, c):
         part = pl.ds(c * step, step)
-        to_far[half, c] = send(
-            weight[half].at[part], wbuf.at[half, 1, part], pair(w_sem, 1, half, c), (far, t)
-        )
         to_side[half, c] = send(
             weight[half].at[part], wbuf.at[half, 0, part], pair(w_sem, 0, half, c), (side, t)
         )
+
+    for half in range(2):
+        for c in range(CHUNKS):
+            part = pl.ds(c * step, step)
+            send_sem, recv_sem = pair(w_sem, 1, half, c)
+            to_far[half, c] = pltpu.make_async_remote_copy(
+                src_ref=weight[half].at[part],
+                dst_ref=wbuf.at[half, 1, part],
+                send_sem=send_sem,
+                recv_sem=recv_sem,
+                device_id=(far, t),
+                device_id_type=MESH,
+            )
+            started.append(to_far[half, c])
+
+    inner = (s // 2) % 2 != s // 4
+
+    def inner_far(*chunks):
+        @pl.when(inner)
+        def _():
+            for chunk in chunks:
+                to_far[chunk].start()
+
+    def outer_far(*chunks):
+        @pl.when(jnp.logical_not(inner))
+        def _():
+            for chunk in chunks:
+                to_far[chunk].start()
 
     def pass_on(half, c):
         part = pl.ds(c * step, step)
@@ -250,8 +269,6 @@
         onward[half, c] = send(
             wbuf.at[half, 1, part], wbuf.at[half, 2, part], pair(w_sem, 2, half, c), (side, t)
         )
-
-    send_chunk(0, 0)
 
     need(3, 4, 5, 1, 2)
     g = (
@@ -299,13 +316,21 @@
     dec[s] = jnp.exp(passed)
     cols[s] = st[s]
 
+    pl.semaphore_wait(barrier, len(greet))
+    need(7, 11)
+    halo_copy = send(
+        x_ref.at[pl.ds(rows - HALO, HALO)], halo, pair(halo_sem), (lax.rem(s + 1, n_sp), t)
+    )
     first = []
     for d in range(1, n_sp):
         dst = lax.rem(s + d, n_sp)
         first.append(send(st.at[dst], cols.at[s], pair(a_sem, d - 1), (dst, t)))
         first.append(send(dec.at[s], dec.at[s], pair(d_sem, d - 1), (dst, t)))
 
-    send_chunk(0, 1)
+    to_far[0, 0].start()
+    over_side(0, 0)
+    over_side(0, 1)
+    inner_far((0, 1))
 
     halo_copy.wait_recv()
     need(8, 9)
@@ -333,7 +358,8 @@
 
     need(10, 0, 6)
     for c in range(CHUNKS):
-        send_chunk(1, c)
+        over_side(1, c)
+    inner_far(*((1, c) for c in range(CHUNKS)))
     mix_copies = {0: send(mix.at[0, 0], mix.at[1, 0], pair(mix_sem, 0), (low, t))}
     pass_on(0, 0)
 
@@ -356,8 +382,7 @@
                 read * scale * gain_ref[...]
             ).astype(bf16)
     mix_copies[1] = send(mix.at[0, 1], mix.at[1, 1], pair(mix_sem, 1), (low, t))
-    for c in range(1, CHUNKS):
-        pass_on(0, c)
+    outer_far((0, 1), *((1, c) for c in range(CHUNKS)))
 
     halves, results = {}, {}
 
@@ -403,6 +428,8 @@
     product(0, 1)
     finish(0, 0)
     finish(0, 1)
+    for c in range(1, CHUNKS):
+        pass_on(0, c)
     for half in range(2):
         mix_copies[half].wait_recv()
     product(1, 0)

time: 58.6 us -> 54.2 us (0.925)
  Pallas kernels: 56.7 us -> 52.3 us
    pallas_call x1, Pallas kernels: 56.7 us -> 52.3 us  [fused(): pl.pallas_call(functools.partial(kernel, n_sp, n_tp), out_shape=jax.Shape...]
where the time goes in v3:
time: 54.2 us; the launch traced here: 54 us
  Pallas kernels  52.3 us (96%)
  local copies, waits for them, and re-layouts  1.67 us (3%)
    pallas_call x1, Pallas kernels, fused(): pl.pallas_call(functools.partial(kernel, n_sp, n_tp), out_shape=jax.Shape...  52.3 us
    unnamed x1, local copies, waits for them, and re-layouts  1.67 us

profile of v3, /device:TPU:0, one launch (start us, length us, event | category | flops | bytes accessed | tf_op | source)
XLA Modules:
  0.0 54.0 jit_solution(9340200693427997701)
XLA Ops:
  0.0 52.3 %shard_map.118 = bf16[64,2048]{1,0:T(8,128)(2,1)} custom-call(bf16[256,256]{1,0:T(8,128)(2,1)} %refs_0_.1, bf16[256,256]{1,0:T(8,128)(2,1)} %refs_1_.1, bf16[256,512]{1,0:T(8,128)(2,1)} %refs_2_.1, bf16[32,256]{1,0:T(8,128)(2,1)} %bitcast.3, bf16[32,256]{1,0:T(8,128)(2,1)} %refs_4_.1, f32[1,256]{1,0:T(1,128)} %bitcast.4, f32[1,256]{1,0:T(1,128)} %bitcast.5, ...), custom_call_target="tpu_custom_call" | custom-call | tf_op jit(solution)/shard_map/pallas_call | solution.py:508
  52.3 1.7 %copy.14 = bf16[64,2048]{1,0:T(8,128)(2,1)} copy(bf16[64,2048]{1,0:T(8,128)(2,1)} %shard_map.118) | data formatting | bytes 524288

commit v4 on v3

--- a/solution.py
+++ b/solution.py
@@ -327,10 +327,8 @@
         first.append(send(st.at[dst], cols.at[s], pair(a_sem, d - 1), (dst, t)))
         first.append(send(dec.at[s], dec.at[s], pair(d_sem, d - 1), (dst, t)))
 
-    to_far[0, 0].start()
+    inner_far((0, 0))
     over_side(0, 0)
-    over_side(0, 1)
-    inner_far((0, 1))
 
     halo_copy.wait_recv()
     need(8, 9)
@@ -357,11 +355,12 @@
         second.append(send(bef.at[dst], inc.at[s], pair(b_sem, d - 1), (dst, t)))
 
     need(10, 0, 6)
+    over_side(0, 1)
+    inner_far((0, 1))
     for c in range(CHUNKS):
         over_side(1, c)
     inner_far(*((1, c) for c in range(CHUNKS)))
     mix_copies = {0: send(mix.at[0, 0], mix.at[1, 0], pair(mix_sem, 0), (low, t))}
-    pass_on(0, 0)
 
     for copy in second:
         copy.wait_recv()
@@ -382,7 +381,7 @@
                 read * scale * gain_ref[...]
             ).astype(bf16)
     mix_copies[1] = send(mix.at[0, 1], mix.at[1, 1], pair(mix_sem, 1), (low, t))
-    outer_far((0, 1), *((1, c) for c in range(CHUNKS)))
+    outer_far(*((h, c) for h in range(2) for c in range(CHUNKS)))
 
     halves, results = {}, {}
 
@@ -428,7 +427,7 @@
     product(0, 1)
     finish(0, 0)
     finish(0, 1)
-    for c in range(1, CHUNKS):
+    for c in range(CHUNKS):
         pass_on(0, c)
     for half in range(2):
         mix_copies[half].wait_recv()

time: 54.2 us -> 53.5 us (0.987)
  Pallas kernels: 52.3 us -> 51.6 us
    pallas_call x1, Pallas kernels: 52.3 us -> 51.6 us  [fused(): pl.pallas_call(functools.partial(kernel, n_sp, n_tp), out_shape=jax.Shape...]
where the time goes in v4:
time: 53.5 us; the launch traced here: 53.3 us
  Pallas kernels  51.6 us (96%)
  local copies, waits for them, and re-layouts  1.67 us (3%)
    pallas_call x1, Pallas kernels, fused(): pl.pallas_call(functools.partial(kernel, n_sp, n_tp), out_shape=jax.Shape...  51.6 us
    unnamed x1, local copies, waits for them, and re-layouts  1.67 us

profile of v4, /device:TPU:0, one launch (start us, length us, event | category | flops | bytes accessed | tf_op | source)
XLA Modules:
  0.0 53.3 jit_solution(7351701295522100054)
XLA Ops:
  0.0 51.6 %shard_map.118 = bf16[64,2048]{1,0:T(8,128)(2,1)} custom-call(bf16[256,256]{1,0:T(8,128)(2,1)} %refs_0_.1, bf16[256,256]{1,0:T(8,128)(2,1)} %refs_1_.1, bf16[256,512]{1,0:T(8,128)(2,1)} %refs_2_.1, bf16[32,256]{1,0:T(8,128)(2,1)} %bitcast.3, bf16[32,256]{1,0:T(8,128)(2,1)} %refs_4_.1, f32[1,256]{1,0:T(1,128)} %bitcast.4, f32[1,256]{1,0:T(1,128)} %bitcast.5, ...), custom_call_target="tpu_custom_call" | custom-call | tf_op jit(solution)/shard_map/pallas_call | solution.py:507
  51.6 1.7 %copy.14 = bf16[64,2048]{1,0:T(8,128)(2,1)} copy(bf16[64,2048]{1,0:T(8,128)(2,1)} %shard_map.118) | data formatting | bytes 524288
